TPU v7x, 32 devices: a whole 2x2x4 slice. The times are simulated.
32 devices in a mesh: sp: 8 (over z, x), tp: 4 (over y, core).
Axes of the slice: x: 2, y: 2, z: 4, core: 2. Of those that a mesh axis runs over, the one named last changes fastest.
Arguments:
- resid: bfloat16 [2048, 4096], P('sp'), may hold values from -6 to 6
- queries: bfloat16 [2048, 3072], P('sp', 'tp'), may hold values from -1000 to 1000
- latent: bfloat16 [2048, 512], P('sp'), may hold values from -6 to 6
- rope_key: bfloat16 [2048, 64], P('sp'), may hold values from -6 to 6
- lat_gain: float32 [512], replicated, may hold values from 0.1 to 1.9
- kv_weight: bfloat16 [512, 4096], P(None, 'tp'), may hold values from -4 to 4
- out_gain: float32 [2048], P('tp'), may hold values from 0.1 to 1.9
- out_weight: bfloat16 [2048, 4096], P('tp'), may hold values from -0.125 to 0.125
- ffn_gain: float32 [4096], replicated, may hold values from 0.1 to 1.9
- gate_weight: bfloat16 [4096, 6144], P('sp', 'tp'), may hold values from -0.09375 to 0.09375
- up_weight: bfloat16 [4096, 6144], P('sp', 'tp'), may hold values from -0.09375 to 0.09375
- down_weight: bfloat16 [6144, 4096], P('tp', 'sp'), may hold values from -0.078125 to 0.078125
Outputs:
- result: bfloat16 [2048, 4096], P(('sp', 'tp'))
All inputs are finite; a program needn't handle non-finite values.
Results may differ from a plain program's by a relative error of at most 0.018.
Values may be sent and summed in bfloat16 or wider, within the bound.
A program may use at most 192 MiB of HBM per device.

v0:
```python
import math

import jax
import jax.numpy as jnp
from jax import lax
from jax.sharding import PartitionSpec as P

HEADS = 16
NOPE = 128
ROPE = 64
VDIM = 128


EPSILON = 1e-06
THETA = 10000.0
LOWEST = -1e30


def rotate(values, places):
    half = values.shape[-1] // 2
    inverse = THETA ** (-jnp.arange(half, dtype=jnp.float32) / half)
    angle = places[..., None] * inverse
    cosine = jnp.cos(angle)
    sine = jnp.sin(angle)
    first = values[..., :half]
    second = values[..., half:]
    return jnp.concatenate(
        [first * cosine - second * sine, first * sine + second * cosine], axis=-1
    )


def norm_rows(values, gain):
    wide = values.astype(jnp.float32)
    return wide * lax.rsqrt(jnp.mean(wide * wide, axis=-1, keepdims=True) + EPSILON) * gain


def make_keys(latent_piece, rotary_piece, lat_gain, kv_weight):
    normed = norm_rows(latent_piece, lat_gain).astype(jnp.bfloat16)
    key_value = jnp.dot(normed, kv_weight, preferred_element_type=jnp.float32).astype(jnp.bfloat16)
    key_index = jnp.arange(latent_piece.shape[0], dtype=jnp.int32)
    key_rope = rotate(rotary_piece.astype(jnp.float32), key_index.astype(jnp.float32)).astype(
        jnp.bfloat16
    )
    return (key_value, key_rope)


def body(
    resid,
    queries,
    latent,
    rope_key,
    lat_gain,
    kv_weight,
    out_gain,
    out_weight,
    ffn_gain,
    gate_weight,
    up_weight,
    down_weight,
):
    rows_here = resid.shape[0]
    first_row = lax.axis_index("sp") * rows_here
    heads_here = queries.shape[1] // (NOPE + ROPE)
    query = queries.reshape(rows_here, heads_here, NOPE + ROPE)
    query_index = first_row + jnp.arange(rows_here, dtype=jnp.int32)
    query_nope = query[:, :, :NOPE]
    query_rope = rotate(
        query[:, :, NOPE:].astype(jnp.float32), query_index.astype(jnp.float32)[:, None]
    ).astype(jnp.bfloat16)
    scale = 1.0 / math.sqrt(NOPE + ROPE)

    def accumulate(state, key_value, key_rope):
        running_max, running_sum, weighted = state
        length = key_value.shape[0]
        key_value = key_value.reshape(length, heads_here, NOPE + VDIM)
        key_index = jnp.arange(length, dtype=jnp.int32)
        scores = jnp.einsum(
            "qhd,khd->hqk", query_nope, key_value[:, :, :NOPE], preferred_element_type=jnp.float32
        )
        scores = (
            scores
            + jnp.einsum("qhr,kr->hqk", query_rope, key_rope, preferred_element_type=jnp.float32)
        ) * scale
        allowed = (key_index[None, :] <= query_index[:, None])[None]
        scores = jnp.where(allowed, scores, LOWEST)
        new_max = jnp.maximum(running_max, jnp.max(scores, axis=-1))
        weights = jnp.where(allowed, jnp.exp(scores - new_max[:, :, None]), 0.0)
        running_sum = jnp.sum(weights, axis=-1)
        added = jnp.einsum(
            "hqk,khd->qhd",
            weights.astype(jnp.bfloat16),
            key_value[:, :, NOPE:],
            preferred_element_type=jnp.float32,
        )
        weighted = added
        return (new_max, running_sum, weighted)

    def unchanged(state):
        return state

    initial = (
        jnp.full((heads_here, rows_here), LOWEST, jnp.float32),
        jnp.zeros((heads_here, rows_here), jnp.float32),
        jnp.zeros((rows_here, heads_here, VDIM), jnp.float32),
    )
    pieces = (
        lax.all_gather(latent, "sp", axis=0, tiled=True),
        lax.all_gather(rope_key, "sp", axis=0, tiled=True),
    )

    def update(state):
        key_value, key_rope = make_keys(pieces[0], pieces[1], lat_gain, kv_weight)
        return accumulate(state, key_value, key_rope)

    running_max, running_sum, weighted = lax.cond(
        jnp.int32(0) < first_row + rows_here, update, unchanged, initial
    )
    attended = (weighted / jnp.transpose(running_sum)[:, :, None]).astype(jnp.bfloat16)
    attended_float = attended.reshape(rows_here, heads_here * VDIM).astype(jnp.float32)
    squares = lax.psum(jnp.sum(attended_float * attended_float, axis=1), "tp")
    normed_out = attended_float * lax.rsqrt(squares / (HEADS * VDIM) + EPSILON)[:, None] * out_gain
    normed_out = normed_out.astype(jnp.bfloat16)
    share = rows_here // lax.axis_size("tp")
    own_first = lax.axis_index("tp") * share
    attn_sum = lax.psum_scatter(
        jnp.dot(normed_out, out_weight, preferred_element_type=jnp.float32).astype(jnp.bfloat16),
        "tp",
        scatter_dimension=0,
        tiled=True,
    ).astype(jnp.float32)
    own_resid = lax.dynamic_slice_in_dim(resid, own_first, share, 0)
    middle = (own_resid.astype(jnp.float32) + attn_sum).astype(jnp.bfloat16)
    normed_mid = lax.all_gather(
        norm_rows(middle, ffn_gain).astype(jnp.bfloat16), "tp", axis=0, tiled=True
    )
    gate = jnp.dot(
        normed_mid,
        lax.all_gather(gate_weight, "sp", axis=0, tiled=True),
        preferred_element_type=jnp.float32,
    )
    upward = jnp.dot(
        normed_mid,
        lax.all_gather(up_weight, "sp", axis=0, tiled=True),
        preferred_element_type=jnp.float32,
    )
    hidden = (jax.nn.silu(gate) * upward).astype(jnp.bfloat16)
    terms = jnp.dot(
        hidden,
        lax.all_gather(down_weight, "sp", axis=1, tiled=True),
        preferred_element_type=jnp.float32,
    )
    ffn_sum = lax.psum_scatter(
        terms.astype(jnp.bfloat16), "tp", scatter_dimension=0, tiled=True
    ).astype(jnp.float32)
    return (middle.astype(jnp.float32) + ffn_sum).astype(jnp.bfloat16)


def solution(mesh):
    placed = (
        P("sp", None),
        P("sp", "tp"),
        P("sp", None),
        P("sp", None),
        P(),
        P(None, "tp"),
        P("tp"),
        P("tp", None),
        P(),
        P("sp", "tp"),
        P("sp", "tp"),
        P("tp", "sp"),
    )
    return jax.shard_map(
        body, mesh=mesh, in_specs=placed, out_specs=P(("sp", "tp"), None), check_vma=False
    )
```

profile of v0, /device:TPU:0, one launch (start us, length us, event | category | flops | bytes accessed | tf_op | source)
XLA Modules:
  0.0 732.7 jit_solution(17946913857392103547)
XLA Ops:
  7.3 1.2 copy.20
  8.5 33.1 %all_gather.19 = bf16[2048,64]{0,1:T(8,128)(2,1)S(1)} all-gather(bf16[256,64]{0,1:T(8,128)(2,1)} %param.17), channel_id=1, replica_groups=mesh['sp'=8,'tp'=4] {'sp'}, dimensions={0}, use_global_device_ids=true | all-gather | bytes 294912 | tf_op jit(solution)/shard_map/all_gather | solution.py:108
  41.9 20.0 %all-gather.6.cloned.1.call-done = bf16[2048,512]{1,0:T(8,128)(2,1)} async-done(((bf16[256,512]{1,0:T(8,128)(2,1)}), bf16[2048,512]{1,0:T(8,128)(2,1)}) %all-gather.6.cloned.1.call-update) | async-done | bytes 2097168 | tf_op jit(solution)/shard_map/all_gather | solution.py:107
  62.0 18.5 %conditional.1 = (f32[4,256]{1,0:T(4,128)S(1)}, f32[256,4,128]{0,2,1:T(8,128)S(1)}) conditional(s32[]{:T(128)} %convert_element_type.90, () %tuple.13, (s32[]{:T(128)}, s32[256]{0:T(256)S(1)}, bf16[2048,512]{1,0:T(8,128)(2,1)}, f32[512]{0:T(512)}, bf16[512,1024]{1,0:T(8,128)(2,1)}, /*index=5*/bf16[256,4,192]{0,2,1:T(8,128)(2,1)S(1)}, ...), branch_computations={%region_0.0_spmd, %region_1.5_spmd} | conditional | flops 3521842432 | bytes 78066992 | solution.py:115
  62.0 2.1 fusion.4
  64.1 6.3 convolution_convert_fusion
  70.6 2.9 fusion.14
  74.0 1.2 fusion.28
  75.1 2.1 fusion.46
  77.3 1.7 fusion.18
  79.0 1.5 fusion.3
  80.6 5.8 psum.7
  86.6 4.8 convolution_convert_fusion.2
  91.5 30.1 %reduce-scatter.3.cloned.1.call-done = bf16[64,4096]{1,0:T(8,128)(2,1)} async-done(((bf16[256,4096]{1,0:T(8,128)(2,1)}), bf16[64,4096]{1,0:T(8,128)(2,1)}) %reduce-scatter.3.cloned.1.call-update) | async-done | bytes 524304 | tf_op jit(solution)/shard_map/reduce_scatter | solution.py:125
  121.7 1.5 fusion.37
  123.2 1.0 fusion.39
  126.0 20.9 %all-gather.8.cloned.1.call-done = bf16[256,4096]{1,0:T(8,128)(2,1)} async-done(((bf16[64,4096]{1,0:T(8,128)(2,1)}), bf16[256,4096]{1,0:T(8,128)(2,1)}) %all-gather.8.cloned.1.call-update) | async-done | bytes 2097168 | tf_op jit(solution)/shard_map/all_gather | solution.py:133
  146.9 178.2 %all-gather.10.cloned.1.call-done = bf16[4096,1536]{1,0:T(8,128)(2,1)} async-done(((bf16[512,1536]{1,0:T(8,128)(2,1)}), bf16[4096,1536]{1,0:T(8,128)(2,1)}) %all-gather.10.cloned.1.call-update) | async-done | bytes 12582928 | tf_op jit(solution)/shard_map/all_gather | solution.py:138
  325.1 9.7 %fusion.47 = f32[256,1536]{1,0:T(8,128)} fusion(bf16[256,4096]{1,0:T(8,128)(2,1)} %all-gather.8.cloned.1.call-done, bf16[4096,1536]{1,0:T(8,128)(2,1)} %all-gather.10.cloned.1.call-done), kind=kOutput, calls=%fused_computation.74 | convolution fusion | flops 3221225472 | bytes 16252928 | tf_op jit(solution)/shard_map/dot_general | solution.py:136
  334.8 166.6 %all-gather.12.cloned.1.call-done = bf16[4096,1536]{1,0:T(8,128)(2,1)} async-done(((bf16[512,1536]{1,0:T(8,128)(2,1)}), bf16[4096,1536]{1,0:T(8,128)(2,1)}) %all-gather.12.cloned.1.call-update) | async-done | bytes 12582928 | tf_op jit(solution)/shard_map/all_gather | solution.py:143
  501.4 176.2 %all-gather.14.cloned.1.call-done = bf16[1536,4096]{1,0:T(8,128)(2,1)} async-done(((bf16[1536,512]{1,0:T(8,128)(2,1)}), bf16[1536,4096]{1,0:T(8,128)(2,1)}) %all-gather.14.cloned.1.call-update) | async-done | bytes 12582928 | tf_op jit(solution)/shard_map/all_gather | solution.py:149
  677.6 16.7 %convolution_convert_fusion.1 = bf16[256,4096]{1,0:T(8,128)(2,1)} fusion(bf16[1536,4096]{1,0:T(8,128)(2,1)} %all-gather.14.cloned.1.call-done, bf16[256,4096]{1,0:T(8,128)(2,1)S(1)} %copy-done.3, bf16[4096,1536]{1,0:T(8,128)(2,1)} %all-gather.12.cloned.1.call-done, f32[256,1536]{1,0:T(8,128)} %fusion.47), kind=kOutput, calls=%fused_computation.44 | convolution fusion | flops 6445858816 | bytes 30932992 | tf_op jit(solution)/shard_map/dot_general | solution.py:147
  694.4 29.5 %reduce-scatter.5.cloned.1.call-done = bf16[64,4096]{1,0:T(8,128)(2,1)} async-done(((bf16[256,4096]{1,0:T(8,128)(2,1)}), bf16[64,4096]{1,0:T(8,128)(2,1)}) %reduce-scatter.5.cloned.1.call-update) | async-done | bytes 524304 | tf_op jit(solution)/shard_map/reduce_scatter | solution.py:152
  723.9 2.0 fusion.40
  (41 shorter events, 3.8 us)
Async XLA Ops:
  6.5 55.4 %all-gather.6.cloned.1.call-start = ((), (), s32[]{:S(2)}) async-start(), calls=%async_computation.2 | async-start | bytes 2359296 | tf_op jit(solution)/shard_map/all_gather | solution.py:107
  7.3 114.4 %reduce-scatter.3.cloned.1.call-start = ((), (), s32[]{:S(2)}) async-start(), calls=%async_computation.3 | async-start | bytes 2621440 | tf_op jit(solution)/shard_map/reduce_scatter | solution.py:125
  62.0 24.5 %copy-start.2 = (f32[512]{0:T(512)S(1)}, f32[512]{0:T(512)}, u32[]{:S(2)}) copy-start(f32[512]{0:T(512)} %param.20) | copy-start | bytes 6148
  75.1 2.2 copy-start
  86.6 36.5 %copy-start.1 = (f32[4096]{0:T(1024)S(1)}, f32[4096]{0:T(1024)}, u32[]{:S(2)}) copy-start(f32[4096]{0:T(1024)} %param.22) | copy-start | bytes 49156
  91.5 55.4 %all-gather.8.cloned.1.call-start = ((), (), s32[]{:S(2)}) async-start(), calls=%async_computation.4 | async-start | bytes 2621440 | tf_op jit(solution)/shard_map/all_gather | solution.py:133
  124.2 200.9 %all-gather.10.cloned.1.call-start = ((), (), s32[]{:S(2)}) async-start(), calls=%async_computation.5 | async-start | bytes 14155776 | tf_op jit(solution)/shard_map/all_gather | solution.py:138
  124.8 376.7 %all-gather.12.cloned.1.call-start = ((), (), s32[]{:S(2)}) async-start(), calls=%async_computation.6 | async-start | bytes 14155776 | tf_op jit(solution)/shard_map/all_gather | solution.py:143
  125.3 552.3 %all-gather.14.cloned.1.call-start = ((), (), s32[]{:S(2)}) async-start(), calls=%async_computation.7 | async-start | bytes 14155776 | tf_op jit(solution)/shard_map/all_gather | solution.py:149
  125.9 598.0 %reduce-scatter.5.cloned.1.call-start = ((), (), s32[]{:S(2)}) async-start(), calls=%async_computation.8 | async-start | bytes 2621440 | tf_op jit(solution)/shard_map/reduce_scatter | solution.py:152
  146.9 530.8 %copy-start.3 = (bf16[256,4096]{1,0:T(8,128)(2,1)S(1)}, bf16[256,4096]{1,0:T(8,128)(2,1)}, u32[]{:S(2)}) copy-start(bf16[256,4096]{1,0:T(8,128)(2,1)} %all-gather.8.cloned.1.call-done) | copy-start | bytes 6291460
Sparse Core Ops, SparseCore 0:
  9.5 52.4 all-gather.5
  91.6 30.0 reduce-scatter.2
  124.3 22.5 all-gather.7
  148.9 176.0 all-gather.9
  327.1 174.2 all-gather.11
  503.3 174.2 all-gather.13
  694.5 29.3 reduce-scatter.4
where the time goes:
time: 733 us
  waiting for transfers between devices  624 us (85%)
  matrix products  44.3 us (6%)
  blocking collectives  39 us (5%)
  between operations  13.6 us (2%)
  other arithmetic  10.1 us (1%)
    all_gather x1, waiting for transfers between devices, body(): lax.all_gather(gate_weight, 'sp', axis=0, tiled=True)  178 us
    all_gather x1, waiting for transfers between devices, body(): lax.all_gather(down_weight, 'sp', axis=1, tiled=True)  176 us
    all_gather x1, waiting for transfers between devices, body(): lax.all_gather(up_weight, 'sp', axis=0, tiled=True)  167 us
    all_gather x1, blocking collectives, body(): lax.all_gather(rope_key, 'sp', axis=0, tiled=True)  33.1 us
    reduce_scatter x1, waiting for transfers between devices, body(): lax.psum_scatter(jnp.dot(normed_out, out_weight, preferred_element_type=j...  30.1 us
    reduce_scatter x1, waiting for transfers between devices, body(): lax.psum_scatter(terms.astype(jnp.bfloat16), 'tp', scatter_dimension=0, t...  29.5 us
    all_gather x1, waiting for transfers between devices, body(): lax.all_gather(norm_rows(middle, ffn_gain).astype(jnp.bfloat16), 'tp', ax...  20.9 us
    all_gather x1, waiting for transfers between devices, body(): lax.all_gather(latent, 'sp', axis=0, tiled=True)  20 us
  transfers between devices with their start and end apart: 7, of which 7 were waited for; matrix products, arithmetic and copies ran while one was open for 2% of the time, Pallas kernels for 0%

commit v1 on v0

--- a/solution.py
+++ b/solution.py
@@ -5,6 +5,7 @@
 from jax import lax
 from jax.sharding import PartitionSpec as P
 
+
 HEADS = 16
 NOPE = 128
 ROPE = 64
@@ -14,6 +15,7 @@
 EPSILON = 1e-06
 THETA = 10000.0
 LOWEST = -1e30
+GROUP = 4
 
 
 def rotate(values, places):
@@ -36,12 +38,61 @@
 
 def make_keys(latent_piece, rotary_piece, lat_gain, kv_weight):
     normed = norm_rows(latent_piece, lat_gain).astype(jnp.bfloat16)
-    key_value = jnp.dot(normed, kv_weight, preferred_element_type=jnp.float32).astype(jnp.bfloat16)
+    key_value = jnp.dot(normed, kv_weight, preferred_element_type=jnp.float32)
+    key_value = key_value.astype(jnp.bfloat16)
     key_index = jnp.arange(latent_piece.shape[0], dtype=jnp.int32)
     key_rope = rotate(rotary_piece.astype(jnp.float32), key_index.astype(jnp.float32)).astype(
         jnp.bfloat16
     )
     return (key_value, key_rope)
+
+
+def to_near(values, flip):
+    ranks = lax.axis_size("sp")
+    return lax.ppermute(values, "sp", [(rank, rank ^ flip) for rank in range(ranks)])
+
+
+def to_high(values, step, ranks):
+    if step % (ranks // GROUP) == 0:
+        return values
+    return lax.ppermute(
+        values, "sp", [(rank, (rank + step * GROUP) % ranks) for rank in range(ranks)]
+    )
+
+
+def by_distance(values, place):
+    blocks = jnp.split(values, GROUP, axis=1)
+    blocks = [jnp.where(place % 2 == 1, blocks[j ^ 1], blocks[j]) for j in range(GROUP)]
+    blocks = [jnp.where(place // 2 == 1, blocks[j ^ 2], blocks[j]) for j in range(GROUP)]
+    return jnp.concatenate(blocks, axis=1)
+
+
+def near_weights(gate, up, down):
+    gate_one = to_near(gate, 1)
+    up_two = to_near(up, 2)
+    up_one = to_near(up, 1)
+    gate_two = to_near(gate, 2)
+    gate_both = to_near(gate_one, 2)
+    up_both = to_near(up_two, 1)
+    down, gate_both, up_both = lax.optimization_barrier((down, gate_both, up_both))
+    half = down.shape[0] // 2
+    down_one = to_near(down, 1)
+    down_two = to_near(down, 2)
+    down_both = jnp.concatenate([to_near(down_one[:half], 2), to_near(down_two[half:], 1)], axis=0)
+    return (
+        (gate, gate_one, gate_two, gate_both),
+        (up, up_one, up_two, up_both),
+        (down, down_one, down_two, down_both),
+    )
+
+
+def blocks_dot(rows, weights, block):
+    return sum(
+        jnp.dot(
+            rows[:, place * block : (place + 1) * block], weight, preferred_element_type=jnp.float32
+        )
+        for place, weight in enumerate(weights)
+    )
 
 
 def body(
@@ -58,6 +109,7 @@
     up_weight,
     down_weight,
 ):
+    gate_blocks, up_blocks, down_blocks = near_weights(gate_weight, up_weight, down_weight)
     rows_here = resid.shape[0]
     first_row = lax.axis_index("sp") * rows_here
     heads_here = queries.shape[1] // (NOPE + ROPE)
@@ -95,26 +147,21 @@
         weighted = added
         return (new_max, running_sum, weighted)
 
-    def unchanged(state):
-        return state
-
     initial = (
         jnp.full((heads_here, rows_here), LOWEST, jnp.float32),
         jnp.zeros((heads_here, rows_here), jnp.float32),
         jnp.zeros((rows_here, heads_here, VDIM), jnp.float32),
     )
-    pieces = (
-        lax.all_gather(latent, "sp", axis=0, tiled=True),
-        lax.all_gather(rope_key, "sp", axis=0, tiled=True),
-    )
+    both = lax.all_gather(
+        jnp.concatenate([latent, rope_key], axis=1), "sp", axis=0, tiled=True
+    )
+    pieces = (both[:, : latent.shape[1]], both[:, latent.shape[1] :])
 
     def update(state):
         key_value, key_rope = make_keys(pieces[0], pieces[1], lat_gain, kv_weight)
         return accumulate(state, key_value, key_rope)
 
-    running_max, running_sum, weighted = lax.cond(
-        jnp.int32(0) < first_row + rows_here, update, unchanged, initial
-    )
+    _, running_sum, weighted = update(initial)
     attended = (weighted / jnp.transpose(running_sum)[:, :, None]).astype(jnp.bfloat16)
     attended_float = attended.reshape(rows_here, heads_here * VDIM).astype(jnp.float32)
     squares = lax.psum(jnp.sum(attended_float * attended_float, axis=1), "tp")
@@ -122,35 +169,72 @@
     normed_out = normed_out.astype(jnp.bfloat16)
     share = rows_here // lax.axis_size("tp")
     own_first = lax.axis_index("tp") * share
+    projected = jnp.dot(normed_out, out_weight, preferred_element_type=jnp.float32)
+    projected = projected.astype(jnp.bfloat16)
     attn_sum = lax.psum_scatter(
-        jnp.dot(normed_out, out_weight, preferred_element_type=jnp.float32).astype(jnp.bfloat16),
+        projected,
         "tp",
         scatter_dimension=0,
         tiled=True,
     ).astype(jnp.float32)
     own_resid = lax.dynamic_slice_in_dim(resid, own_first, share, 0)
     middle = (own_resid.astype(jnp.float32) + attn_sum).astype(jnp.bfloat16)
-    normed_mid = lax.all_gather(
-        norm_rows(middle, ffn_gain).astype(jnp.bfloat16), "tp", axis=0, tiled=True
-    )
-    gate = jnp.dot(
-        normed_mid,
-        lax.all_gather(gate_weight, "sp", axis=0, tiled=True),
-        preferred_element_type=jnp.float32,
-    )
-    upward = jnp.dot(
-        normed_mid,
-        lax.all_gather(up_weight, "sp", axis=0, tiled=True),
-        preferred_element_type=jnp.float32,
-    )
-    hidden = (jax.nn.silu(gate) * upward).astype(jnp.bfloat16)
-    terms = jnp.dot(
-        hidden,
-        lax.all_gather(down_weight, "sp", axis=1, tiled=True),
-        preferred_element_type=jnp.float32,
-    )
-    ffn_sum = lax.psum_scatter(
-        terms.astype(jnp.bfloat16), "tp", scatter_dimension=0, tiled=True
+    ranks = lax.axis_size("sp")
+    highs = ranks // GROUP
+    rank = lax.axis_index("sp")
+    high = rank // GROUP
+    place = rank % GROUP
+    width = resid.shape[1]
+    block = width // ranks
+    wide = GROUP * block
+    mids = norm_rows(middle, ffn_gain).astype(jnp.bfloat16)
+    mids = [
+        to_high(
+            by_distance(
+                lax.dynamic_slice_in_dim(mids, (high + step) % highs * wide, wide, 1), place
+            ),
+            step,
+            ranks,
+        )
+        for step in range(highs)
+    ]
+    mids = lax.all_gather(jnp.concatenate(mids, axis=1), "tp", axis=0, tiled=True)
+    gates, ups = None, None
+    for step in list(range(1, highs)) + [0]:
+        piece = mids[:, step * wide : (step + 1) * wide]
+        gate = blocks_dot(piece, gate_blocks, block)
+        up = blocks_dot(piece, up_blocks, block)
+        if step:
+            gate = to_high(gate.astype(jnp.bfloat16), highs - step, ranks).astype(jnp.float32)
+            up = to_high(up.astype(jnp.bfloat16), highs - step, ranks).astype(jnp.float32)
+        gates = gate if gates is None else gates + gate
+        ups = up if ups is None else ups + up
+    hidden = (jax.nn.silu(gates) * ups).astype(jnp.bfloat16)
+    terms = []
+    for step in range(highs):
+        theirs = to_high(hidden, step, ranks)
+        terms += [
+            jnp.dot(theirs, weight, preferred_element_type=jnp.float32).astype(jnp.bfloat16)
+            for weight in down_blocks
+        ]
+    terms = lax.psum_scatter(
+        jnp.concatenate(terms, axis=1), "tp", scatter_dimension=0, tiled=True
+    )
+    terms = jnp.concatenate(
+        [
+            by_distance(
+                to_high(terms[:, step * wide : (step + 1) * wide], highs - step, ranks), place
+            )
+            for step in range(highs)
+        ],
+        axis=1,
+    )
+    ffn_sum = jnp.concatenate(
+        [
+            lax.dynamic_slice_in_dim(terms, (index - high + highs) % highs * wide, wide, 1)
+            for index in range(highs)
+        ],
+        axis=1,
     ).astype(jnp.float32)
     return (middle.astype(jnp.float32) + ffn_sum).astype(jnp.bfloat16)
 
@@ -170,6 +254,7 @@
         P("sp", "tp"),
         P("tp", "sp"),
     )
+
     return jax.shard_map(
         body, mesh=mesh, in_specs=placed, out_specs=P(("sp", "tp"), None), check_vma=False
     )

time: 733 us -> 434 us (0.59)
  waiting for transfers between devices: 624 us -> 317 us
  blocking collectives: 39 us -> 6.04 us
  starting transfers between devices: 0.24 us -> 18.7 us
  matrix products: 44.3 us -> 56.9 us
    all_gather x5 -> x2, waiting for transfers between devices: 562 us -> 55.5 us  [the longest x1 55.4 us: body(): lax.all_gather(jnp.concatenate([latent, rope_key], axis=1), 'sp', axis=0,...]
    ppermute x0 -> x15, waiting for transfers between devices: none -> 231 us  [the longest x5 117 us: to_high(): lax.ppermute(values, 'sp', [(rank, (rank + step * GROUP) % ranks) for ran...]
    all_gather x1 -> x0, blocking collectives: 33.1 us -> none  [body(): lax.all_gather(rope_key, 'sp', axis=0, tiled=True)]
    reduce_scatter x2, waiting for transfers between devices: 59.6 us -> 30.5 us  [the longest x1 30.5 us: body(): lax.psum_scatter(jnp.concatenate(terms, axis=1), 'tp', scatter_dimension=...]
    ppermute x0 -> x15, starting transfers between devices: none -> 18.6 us  [the longest x10 11.5 us: to_near(): lax.ppermute(values, 'sp', [(rank, rank ^ flip) for rank in range(ranks)])]
    dot_general x3 -> x25, matrix products: 32.8 us -> 47 us  [the longest x16 29.5 us: blocks_dot(): jnp.dot(rows[:, place * block:(place + 1) * block], weight, preferred_ele...]
  transfers between devices with their start and end apart: 7 -> 19, of which waited for: 7 -> 13; matrix products, arithmetic and copies ran while one was open for 2% -> 9% of each run, Pallas kernels for 0% -> 0%
where the time goes in v1:
time: 434 us; the launch traced here: 433 us
  waiting for transfers between devices  317 us (73%)
  matrix products  56.9 us (13%)
  starting transfers between devices  18.7 us (4%)
  other arithmetic  14 us (3%)
  between operations  13.7 us (3%)
  local copies, waits for them, and re-layouts  6.87 us (2%)
  blocking collectives  6.04 us (1%)
    ppermute x5, waiting for transfers between devices, to_high(): lax.ppermute(values, 'sp', [(rank, (rank + step * GROUP) % ranks) for ran...  117 us
    ppermute x10, waiting for transfers between devices, to_near(): lax.ppermute(values, 'sp', [(rank, rank ^ flip) for rank in range(ranks)])  114 us
    all_gather x1, waiting for transfers between devices, body(): lax.all_gather(jnp.concatenate([latent, rope_key], axis=1), 'sp', axis=0,...  55.4 us
    reduce_scatter x1, waiting for transfers between devices, body(): lax.psum_scatter(jnp.concatenate(terms, axis=1), 'tp', scatter_dimension=...  30.5 us
    dot_general x16, matrix products, blocks_dot(): jnp.dot(rows[:, place * block:(place + 1) * block], weight, preferred_ele...  29.5 us
    dot_general x8, matrix products, body(): jnp.dot(theirs, weight, preferred_element_type=jnp.float32)  13.4 us
    ppermute x10, starting transfers between devices, to_near(): lax.ppermute(values, 'sp', [(rank, rank ^ flip) for rank in range(ranks)])  11.5 us
  transfers between devices with their start and end apart: 19, of which 13 were waited for; matrix products, arithmetic and copies ran while one was open for 9% of the time, Pallas kernels for 0%

profile of v1, /device:TPU:0, one launch (start us, length us, event | category | flops | bytes accessed | tf_op | source)
XLA Modules:
  0.0 432.9 jit_solution(1305267941352877743)
XLA Ops:
  10.2 55.4 %all-gather.3.cloned.1.call-done = bf16[2048,576]{0,1:T(8,128)(2,1)} async-done(((bf16[256,576]{0,1:T(8,128)(2,1)}), bf16[2048,576]{0,1:T(8,128)(2,1)}) %all-gather.3.cloned.1.call-update) | async-done | bytes 2359312 | tf_op jit(solution)/shard_map/all_gather | solution.py:155
  67.7 4.1 convolution_convert_fusion.1
  75.3 2.1 fusion.104
  80.7 6.0 %psum.7 = f32[256]{0:T(256)S(1)} all-reduce(f32[256]{0:T(256)S(1)} %get-tuple-element.28), channel_id=1, replica_groups=mesh['sp'=8,'tp'=4] {'tp'}, use_global_device_ids=true, to_apply=%region_4.5 | all-reduce | flops 256 | bytes 2048 | tf_op jit(solution)/shard_map/psum | solution.py:167
  86.9 4.8 %convolution_convert_fusion = bf16[256,4096]{1,0:T(8,128)(2,1)} fusion(bf16[256,512]{0,1:T(8,128)(2,1)S(1)} %fusion.60, bf16[512,4096]{1,0:T(8,128)(2,1)} %param.19), kind=kOutput, calls=%fused_computation.8 | convolution fusion | flops 1074790400 | bytes 6553600 | tf_op jit(solution)/shard_map/dot_general | solution.py:172
  93.1 2.5 collective-permute-start.1
  95.5 33.6 %collective-permute-done.1 = bf16[512,1536]{1,0:T(8,128)(2,1)} collective-permute-done((bf16[512,1536]{1,0:T(8,128)(2,1)S(1)}, bf16[512,1536]{1,0:T(8,128)(2,1)}, u32[]{:S(2)}, u32[]{:S(2)}) %collective-permute-start.1) | collective-permute-done | bytes 1572896 | tf_op jit(solution)/shard_map/ppermute | solution.py:52
  134.7 32.8 %collective-permute-done = bf16[64,2048]{1,0:T(8,128)(2,1)S(1)} collective-permute-done((bf16[64,2048]{1,0:T(8,128)(2,1)S(1)}, bf16[64,2048]{1,0:T(8,128)(2,1)S(1)}, u32[]{:S(2)}, u32[]{:S(2)}) %collective-permute-start) | collective-permute-done | bytes 262176 | tf_op jit(solution)/shard_map/ppermute | solution.py:58
  170.7 2.5 collective-permute-start.10
  173.2 30.8 %collective-permute-done.9 = bf16[1536,512]{1,0:T(8,128)(2,1)S(1)} collective-permute-done((bf16[1536,512]{1,0:T(8,128)(2,1)}, bf16[1536,512]{1,0:T(8,128)(2,1)S(1)}, u32[]{:S(2)}, u32[]{:S(2)}) %collective-permute-start.9) | collective-permute-done | bytes 1572896 | tf_op jit(solution)/shard_map/ppermute | solution.py:52
  204.0 3.1 collective-permute-start.11
  210.8 45.4 %collective-permute-done.11 = bf16[768,512]{1,0:T(8,128)(2,1)S(1)} collective-permute-done((bf16[768,512]{1,0:T(8,128)(2,1)S(1)}, bf16[768,512]{1,0:T(8,128)(2,1)S(1)}, u32[]{:S(2)}, u32[]{:S(2)}) %collective-permute-start.11) | collective-permute-done | bytes 786464 | tf_op jit(solution)/shard_map/ppermute | solution.py:52
  258.1 2.2 fusion.94
  273.8 2.2 collective-permute-start.8
  284.6 2.0 fusion.13
  286.7 30.6 %collective-permute-done.6 = bf16[256,1536]{1,0:T(8,128)(2,1)S(1)} collective-permute-done((bf16[256,1536]{1,0:T(8,128)(2,1)S(1)}, bf16[256,1536]{1,0:T(8,128)(2,1)S(1)}, u32[]{:S(2)}, u32[]{:S(2)}) %collective-permute-start.6) | collective-permute-done | bytes 786464 | tf_op jit(solution)/shard_map/ppermute | solution.py:58
  319.3 13.9 %collective-permute-done.8 = bf16[256,1536]{1,0:T(8,128)(2,1)S(1)} collective-permute-done((bf16[256,1536]{1,0:T(8,128)(2,1)S(1)}, bf16[256,1536]{1,0:T(8,128)(2,1)S(1)}, u32[]{:S(2)}, u32[]{:S(2)}) %collective-permute-start.8) | collective-permute-done | bytes 786464 | tf_op jit(solution)/shard_map/ppermute | solution.py:58
  333.2 2.2 multiply_convert_fusion
  339.5 2.7 fusion.36
  342.2 30.2 %collective-permute-done.13 = bf16[256,1536]{1,0:T(8,128)(2,1)S(1)} collective-permute-done((bf16[256,1536]{1,0:T(8,128)(2,1)S(1)}, bf16[256,1536]{1,0:T(8,128)(2,1)S(1)}, u32[]{:S(2)}, u32[]{:S(2)}) %collective-permute-start.13) | collective-permute-done | bytes 786464 | tf_op jit(solution)/shard_map/ppermute | solution.py:58
  376.4 2.7 fusion.32
  379.1 30.5 %reduce-scatter.5.cloned.1.call-done = bf16[64,4096]{1,0:T(8,128)(2,1)} async-done(((bf16[256,4096]{1,0:T(8,128)(2,1)}), bf16[64,4096]{1,0:T(8,128)(2,1)}) %reduce-scatter.5.cloned.1.call-update) | async-done | bytes 524304 | tf_op jit(solution)/shard_map/reduce_scatter | solution.py:220
  410.7 2.5 collective-permute-start.14
  416.1 9.0 %collective-permute-done.14 = bf16[64,2048]{1,0:T(8,128)(2,1)S(1)} collective-permute-done((bf16[64,2048]{1,0:T(8,128)(2,1)S(1)}, bf16[64,2048]{1,0:T(8,128)(2,1)S(1)}, u32[]{:S(2)}, u32[]{:S(2)}) %collective-permute-start.14) | collective-permute-done | bytes 262176 | tf_op jit(solution)/shard_map/ppermute | solution.py:58
  (121 shorter events, 65.2 us)
Async XLA Ops:
  6.5 61.2 %copy-start = (bf16[512,1024]{1,0:T(8,128)(2,1)S(1)}, bf16[512,1024]{1,0:T(8,128)(2,1)}, u32[]{:S(2)}) copy-start(bf16[512,1024]{1,0:T(8,128)(2,1)} %param.17) | copy-start | bytes 3145732
  6.5 59.1 %all-gather.3.cloned.1.call-start = ((), (), s32[]{:S(2)}) async-start(), calls=%async_computation.2 | async-start | bytes 2654208 | tf_op jit(solution)/shard_map/all_gather | solution.py:155
  9.3 121.8 %reduce-scatter.3.cloned.1.call-start = ((), (), s32[]{:S(2)}) async-start(), calls=%async_computation.3 | async-start | bytes 2621440 | tf_op jit(solution)/shard_map/reduce_scatter | solution.py:174
  9.8 57.9 %copy-start.14 = (f32[512]{0:T(512)S(1)}, f32[512]{0:T(512)}, u32[]{:S(2)}) copy-start(f32[512]{0:T(512)} %param.16) | copy-start | bytes 6148
  91.7 40.9 %copy-start.11 = (f32[4096]{0:T(1024)S(1)}, f32[4096]{0:T(1024)}, u32[]{:S(2)}) copy-start(f32[4096]{0:T(1024)} %param.20) | copy-start | bytes 49156
  91.7 166.4 %all-gather.5.cloned.1.call-start = ((), (), s32[]{:S(2)}) async-start(), calls=%async_computation.4 | async-start | bytes 2621440 | tf_op jit(solution)/shard_map/all_gather | solution.py:201
  93.1 36.1 %collective-permute-start.1 = (bf16[512,1536]{1,0:T(8,128)(2,1)S(1)}, bf16[512,1536]{1,0:T(8,128)(2,1)}, u32[]{:S(2)}, u32[]{:S(2)}) collective-permute-start(bf16[512,1536]{1,0:T(8,128)(2,1)S(1)} %copy-done.3), channel_id=1, source_target_pairs={{0,4},{4,0},{8,12},{12,8},{16,20},{20,16},{24,28},{28,24},{1,5},{5... | collective-permute-start | bytes 4718600 | tf_op jit(solution)/shard_map/ppermute | solution.py:52
  95.5 35.1 %collective-permute-start.4 = (bf16[512,1536]{1,0:T(8,128)(2,1)}, bf16[512,1536]{1,0:T(8,128)(2,1)}, u32[]{:S(2)}, u32[]{:S(2)}) collective-permute-start(bf16[512,1536]{1,0:T(8,128)(2,1)} %param.22), channel_id=1, source_target_pairs={{0,8},{4,12},{8,0},{12,4},{16,24},{20,28},{24,16},{28,20},{1,9},{5... | collective-permute-start | bytes 4718600 | tf_op jit(solution)/shard_map/ppermute | solution.py:52
  129.1 40.7 %collective-permute-start.3 = (bf16[512,1536]{1,0:T(8,128)(2,1)}, bf16[512,1536]{1,0:T(8,128)(2,1)}, u32[]{:S(2)}, u32[]{:S(2)}) collective-permute-start(bf16[512,1536]{1,0:T(8,128)(2,1)} %collective-permute-done.1), channel_id=1, source_target_pairs={{0,8},{4,12},{8,0},{12,4},{16,24},{20,28},{24,16},{28,20},{1,9},{5... | collective-permute-start | bytes 4718600 | tf_op jit(solution)/shard_map/ppermute | solution.py:52
  130.6 39.2 %collective-permute-start.5 = (bf16[512,1536]{1,0:T(8,128)(2,1)}, bf16[512,1536]{1,0:T(8,128)(2,1)}, u32[]{:S(2)}, u32[]{:S(2)}) collective-permute-start(bf16[512,1536]{1,0:T(8,128)(2,1)} %collective-permute-done.4), channel_id=1, source_target_pairs={{0,4},{4,0},{8,12},{12,8},{16,20},{20,16},{24,28},{28,24},{1,5},{5... | collective-permute-start | bytes 4718600 | tf_op jit(solution)/shard_map/ppermute | solution.py:52
  133.0 34.5 %collective-permute-start = (bf16[64,2048]{1,0:T(8,128)(2,1)S(1)}, bf16[64,2048]{1,0:T(8,128)(2,1)S(1)}, u32[]{:S(2)}, u32[]{:S(2)}) collective-permute-start(bf16[64,2048]{1,0:T(8,128)(2,1)S(1)} %pad_maximum_fusion.1), channel_id=1, source_target_pairs={{0,16},{4,20},{8,24},{12,28},{16,0},{20,4},{24,8},{28,12},{1,17},{... | collective-permute-start | bytes 786440 | tf_op jit(solution)/shard_map/ppermute | solution.py:58
  168.4 241.2 %reduce-scatter.5.cloned.1.call-start = ((), (), s32[]{:S(2)}) async-start(), calls=%async_computation.5 | async-start | bytes 2621440 | tf_op jit(solution)/shard_map/reduce_scatter | solution.py:220
  169.9 34.1 %collective-permute-start.9 = (bf16[1536,512]{1,0:T(8,128)(2,1)}, bf16[1536,512]{1,0:T(8,128)(2,1)S(1)}, u32[]{:S(2)}, u32[]{:S(2)}) collective-permute-start(bf16[1536,512]{1,0:T(8,128)(2,1)} %param.23), channel_id=1, source_target_pairs={{0,4},{4,0},{8,12},{12,8},{16,20},{20,16},{24,28},{28,24},{1,5},{5... | collective-permute-start | bytes 4718600 | tf_op jit(solution)/shard_map/ppermute | solution.py:52
  170.7 38.0 %collective-permute-start.10 = (bf16[1536,512]{1,0:T(8,128)(2,1)}, bf16[1536,512]{1,0:T(8,128)(2,1)S(1)}, u32[]{:S(2)}, u32[]{:S(2)}) collective-permute-start(bf16[1536,512]{1,0:T(8,128)(2,1)} %param.23), channel_id=1, source_target_pairs={{0,8},{4,12},{8,0},{12,4},{16,24},{20,28},{24,16},{28,20},{1,9},{5... | collective-permute-start | bytes 4718600 | tf_op jit(solution)/shard_map/ppermute | solution.py:52
  173.1 87.2 %collective-permute-start.2 = (bf16[512,1536]{1,0:T(8,128)(2,1)S(1)}, bf16[512,1536]{1,0:T(8,128)(2,1)}, u32[]{:S(2)}, u32[]{:S(2)}) collective-permute-start(bf16[512,1536]{1,0:T(8,128)(2,1)S(1)} %copy-done.3), channel_id=1, source_target_pairs={{0,8},{4,12},{8,0},{12,4},{16,24},{20,28},{24,16},{28,20},{1,9},{5... | collective-permute-start | bytes 4718600 | tf_op jit(solution)/shard_map/ppermute | solution.py:52
  204.0 52.2 %collective-permute-start.11 = (bf16[768,512]{1,0:T(8,128)(2,1)S(1)}, bf16[768,512]{1,0:T(8,128)(2,1)S(1)}, u32[]{:S(2)}, u32[]{:S(2)}) collective-permute-start(bf16[768,512]{1,0:T(8,128)(2,1)S(1)} %slice.125), channel_id=1, source_target_pairs={{0,8},{4,12},{8,0},{12,4},{16,24},{20,28},{24,16},{28,20},{1,9},{5... | collective-permute-start | bytes 2359304 | tf_op jit(solution)/shard_map/ppermute | solution.py:52
  208.6 48.5 %copy-start.8 = (bf16[1536,512]{1,0:T(8,128)(2,1)}, bf16[1536,512]{1,0:T(8,128)(2,1)S(1)}, u32[]{:S(2)}) copy-start(bf16[1536,512]{1,0:T(8,128)(2,1)S(1)} %collective-permute-done.10) | copy-start | bytes 4718596
  208.7 48.5 %collective-permute-start.12 = (bf16[768,512]{1,0:T(8,128)(2,1)S(1)}, bf16[768,512]{1,0:T(8,128)(2,1)S(1)}, u32[]{:S(2)}, u32[]{:S(2)}) collective-permute-start(bf16[768,512]{1,0:T(8,128)(2,1)S(1)} %slice.126), channel_id=1, source_target_pairs={{0,4},{4,0},{8,12},{12,8},{16,20},{20,16},{24,28},{28,24},{1,5},{5... | collective-permute-start | bytes 2359304 | tf_op jit(solution)/shard_map/ppermute | solution.py:52
  210.2 57.6 %collective-permute-start.7 = (bf16[512,1536]{1,0:T(8,128)(2,1)}, bf16[512,1536]{1,0:T(8,128)(2,1)}, u32[]{:S(2)}, u32[]{:S(2)}) collective-permute-start(bf16[512,1536]{1,0:T(8,128)(2,1)} %param.22), channel_id=1, source_target_pairs={{0,4},{4,0},{8,12},{12,8},{16,20},{20,16},{24,28},{28,24},{1,5},{5... | collective-permute-start | bytes 4718600 | tf_op jit(solution)/shard_map/ppermute | solution.py:52
  265.0 52.3 %collective-permute-start.6 = (bf16[256,1536]{1,0:T(8,128)(2,1)S(1)}, bf16[256,1536]{1,0:T(8,128)(2,1)S(1)}, u32[]{:S(2)}, u32[]{:S(2)}) collective-permute-start(bf16[256,1536]{1,0:T(8,128)(2,1)S(1)} %fusion.18), channel_id=1, source_target_pairs={{0,16},{4,20},{8,24},{12,28},{16,0},{20,4},{24,8},{28,12},{1,17},{... | collective-permute-start | bytes 2359304 | tf_op jit(solution)/shard_map/ppermute | solution.py:58
  273.8 59.4 %collective-permute-start.8 = (bf16[256,1536]{1,0:T(8,128)(2,1)S(1)}, bf16[256,1536]{1,0:T(8,128)(2,1)S(1)}, u32[]{:S(2)}, u32[]{:S(2)}) collective-permute-start(bf16[256,1536]{1,0:T(8,128)(2,1)S(1)} %fusion.19), channel_id=1, source_target_pairs={{0,16},{4,20},{8,24},{12,28},{16,0},{20,4},{24,8},{28,12},{1,17},{... | collective-permute-start | bytes 2359304 | tf_op jit(solution)/shard_map/ppermute | solution.py:58
  319.3 16.1 %copy-start.13 = (bf16[1536,512]{1,0:T(8,128)(2,1)S(1)}, bf16[1536,512]{1,0:T(8,128)(2,1)}, u32[]{:S(2)}) copy-start(bf16[1536,512]{1,0:T(8,128)(2,1)} %param.23) | copy-start | bytes 4718596
  336.7 35.7 %collective-permute-start.13 = (bf16[256,1536]{1,0:T(8,128)(2,1)S(1)}, bf16[256,1536]{1,0:T(8,128)(2,1)S(1)}, u32[]{:S(2)}, u32[]{:S(2)}) collective-permute-start(bf16[256,1536]{1,0:T(8,128)(2,1)S(1)} %multiply_convert_fusion), channel_id=1, source_target_pairs={{0,16},{4,20},{8,24},{12,28},{16,0},{20,4},{24,8},{28,12},{1,17},{... | collective-permute-start | bytes 2359304 | tf_op jit(solution)/shard_map/ppermute | solution.py:58
  410.7 14.5 %collective-permute-start.14 = (bf16[64,2048]{1,0:T(8,128)(2,1)S(1)}, bf16[64,2048]{1,0:T(8,128)(2,1)S(1)}, u32[]{:S(2)}, u32[]{:S(2)}) collective-permute-start(bf16[64,2048]{1,0:T(8,128)(2,1)S(1)} %slice.127), channel_id=1, source_target_pairs={{0,16},{4,20},{8,24},{12,28},{16,0},{20,4},{24,8},{28,12},{1,17},{... | collective-permute-start | bytes 786440 | tf_op jit(solution)/shard_map/ppermute | solution.py:58
  (10 other events, 28.7 us)
Sparse Core Ops, SparseCore 0:
  9.4 56.2 all-gather.2
  91.8 29.4 reduce-scatter.2
  168.5 23.7 all-gather.4
  379.2 30.3 reduce-scatter.4

commit v2 on v1

--- a/solution.py
+++ b/solution.py
@@ -36,11 +36,10 @@
     return wide * lax.rsqrt(jnp.mean(wide * wide, axis=-1, keepdims=True) + EPSILON) * gain
 
 
-def make_keys(latent_piece, rotary_piece, lat_gain, kv_weight):
+def make_keys(latent_piece, rotary_piece, lat_gain, kv_weight, key_index):
     normed = norm_rows(latent_piece, lat_gain).astype(jnp.bfloat16)
     key_value = jnp.dot(normed, kv_weight, preferred_element_type=jnp.float32)
     key_value = key_value.astype(jnp.bfloat16)
-    key_index = jnp.arange(latent_piece.shape[0], dtype=jnp.int32)
     key_rope = rotate(rotary_piece.astype(jnp.float32), key_index.astype(jnp.float32)).astype(
         jnp.bfloat16
     )
@@ -60,11 +59,51 @@
     )
 
 
+def reorder(blocks, place):
+    bit = 1
+    while bit < len(blocks):
+        swap = place // bit % 2 == 1
+        blocks = [jnp.where(swap, blocks[j ^ bit], blocks[j]) for j in range(len(blocks))]
+        bit *= 2
+    return blocks
+
+
 def by_distance(values, place):
-    blocks = jnp.split(values, GROUP, axis=1)
-    blocks = [jnp.where(place % 2 == 1, blocks[j ^ 1], blocks[j]) for j in range(GROUP)]
-    blocks = [jnp.where(place // 2 == 1, blocks[j ^ 2], blocks[j]) for j in range(GROUP)]
-    return jnp.concatenate(blocks, axis=1)
+    return jnp.concatenate(reorder(jnp.split(values, GROUP, axis=1), place), axis=1)
+
+
+def to_column(values, bit):
+    columns = lax.axis_size("tp")
+    return lax.ppermute(values, "tp", [(column, column ^ bit) for column in range(columns)])
+
+
+def gather_columns(values):
+    rows = values.shape[0]
+    held = {0: values}
+    bit = lax.axis_size("tp") // 2
+    while bit:
+        keys = sorted(held)
+        theirs = to_column(jnp.concatenate([held[key] for key in keys], axis=0), bit)
+        for at, key in enumerate(keys):
+            held[key + bit] = theirs[at * rows : (at + 1) * rows]
+        bit //= 2
+    return jnp.concatenate([held[key] for key in sorted(held)], axis=0)
+
+
+def scatter_columns(values):
+    columns = lax.axis_size("tp")
+    blocks = dict(enumerate(jnp.split(values, columns, axis=0)))
+    bit = 1
+    while bit < columns:
+        mine = [key for key in sorted(blocks) if not key & bit]
+        theirs = to_column(jnp.concatenate([blocks[key + bit] for key in mine], axis=0), bit)
+        theirs = jnp.split(theirs, len(mine), axis=0)
+        blocks = {
+            key: (blocks[key].astype(jnp.float32) + piece.astype(jnp.float32)).astype(jnp.bfloat16)
+            for key, piece in zip(mine, theirs)
+        }
+        bit *= 2
+    return blocks[0]
 
 
 def near_weights(gate, up, down):
@@ -78,7 +117,8 @@
     half = down.shape[0] // 2
     down_one = to_near(down, 1)
     down_two = to_near(down, 2)
-    down_both = jnp.concatenate([to_near(down_one[:half], 2), to_near(down_two[half:], 1)], axis=0)
+    far = [to_near(down_one[:half], 2), to_near(down_two[half:], 1)]
+    down_both = jnp.concatenate(far, axis=0)
     return (
         (gate, gate_one, gate_two, gate_both),
         (up, up_one, up_two, up_both),
@@ -113,8 +153,14 @@
     rows_here = resid.shape[0]
     first_row = lax.axis_index("sp") * rows_here
     heads_here = queries.shape[1] // (NOPE + ROPE)
-    query = queries.reshape(rows_here, heads_here, NOPE + ROPE)
-    query_index = first_row + jnp.arange(rows_here, dtype=jnp.int32)
+    columns = lax.axis_size("tp")
+    column = lax.axis_index("tp")
+    share = rows_here // columns
+    query = jnp.concatenate(reorder(jnp.split(queries, columns, axis=0), column), axis=0)
+    query = query.reshape(rows_here, heads_here, NOPE + ROPE)
+    within = jnp.arange(rows_here, dtype=jnp.int32)
+    own_columns = (within // share) ^ column
+    query_index = first_row + own_columns * share + within % share
     query_nope = query[:, :, :NOPE]
     query_rope = rotate(
         query[:, :, NOPE:].astype(jnp.float32), query_index.astype(jnp.float32)[:, None]
@@ -125,7 +171,6 @@
         running_max, running_sum, weighted = state
         length = key_value.shape[0]
         key_value = key_value.reshape(length, heads_here, NOPE + VDIM)
-        key_index = jnp.arange(length, dtype=jnp.int32)
         scores = jnp.einsum(
             "qhd,khd->hqk", query_nope, key_value[:, :, :NOPE], preferred_element_type=jnp.float32
         )
@@ -152,36 +197,39 @@
         jnp.zeros((heads_here, rows_here), jnp.float32),
         jnp.zeros((rows_here, heads_here, VDIM), jnp.float32),
     )
-    both = lax.all_gather(
-        jnp.concatenate([latent, rope_key], axis=1), "sp", axis=0, tiled=True
-    )
+    ranks = lax.axis_size("sp")
+    rank = lax.axis_index("sp")
+    both = jnp.concatenate([latent, rope_key], axis=1)
+    both = lax.dynamic_slice_in_dim(both, column * share, share, 0)
+    pieces = [both]
+    for step in range(1, ranks):
+        onward = [(source, source + step) for source in range(ranks - step)]
+        pieces.append(lax.ppermute(both, "sp", onward))
+    both = gather_columns(jnp.concatenate(pieces, axis=0))
+    within = jnp.arange(both.shape[0], dtype=jnp.int32)
+    source = (rank - within // share % ranks + ranks) % ranks
+    key_index = source * rows_here + ((within // (share * ranks)) ^ column) * share + within % share
     pieces = (both[:, : latent.shape[1]], both[:, latent.shape[1] :])
 
     def update(state):
-        key_value, key_rope = make_keys(pieces[0], pieces[1], lat_gain, kv_weight)
+        key_value, key_rope = make_keys(pieces[0], pieces[1], lat_gain, kv_weight, key_index)
         return accumulate(state, key_value, key_rope)
 
     _, running_sum, weighted = update(initial)
     attended = (weighted / jnp.transpose(running_sum)[:, :, None]).astype(jnp.bfloat16)
     attended_float = attended.reshape(rows_here, heads_here * VDIM).astype(jnp.float32)
-    squares = lax.psum(jnp.sum(attended_float * attended_float, axis=1), "tp")
+    squares = jnp.split(jnp.sum(attended_float * attended_float, axis=1), columns)
+    squares = lax.psum(jnp.concatenate(reorder(squares, column)), "tp")
+    squares = jnp.concatenate(reorder(jnp.split(squares, columns), column))
     normed_out = attended_float * lax.rsqrt(squares / (HEADS * VDIM) + EPSILON)[:, None] * out_gain
     normed_out = normed_out.astype(jnp.bfloat16)
-    share = rows_here // lax.axis_size("tp")
     own_first = lax.axis_index("tp") * share
     projected = jnp.dot(normed_out, out_weight, preferred_element_type=jnp.float32)
     projected = projected.astype(jnp.bfloat16)
-    attn_sum = lax.psum_scatter(
-        projected,
-        "tp",
-        scatter_dimension=0,
-        tiled=True,
-    ).astype(jnp.float32)
+    attn_sum = scatter_columns(projected).astype(jnp.float32)
     own_resid = lax.dynamic_slice_in_dim(resid, own_first, share, 0)
     middle = (own_resid.astype(jnp.float32) + attn_sum).astype(jnp.bfloat16)
-    ranks = lax.axis_size("sp")
     highs = ranks // GROUP
-    rank = lax.axis_index("sp")
     high = rank // GROUP
     place = rank % GROUP
     width = resid.shape[1]
@@ -198,10 +246,10 @@
         )
         for step in range(highs)
     ]
-    mids = lax.all_gather(jnp.concatenate(mids, axis=1), "tp", axis=0, tiled=True)
+    mids = [gather_columns(piece) for piece in mids]
     gates, ups = None, None
     for step in list(range(1, highs)) + [0]:
-        piece = mids[:, step * wide : (step + 1) * wide]
+        piece = mids[step]
         gate = blocks_dot(piece, gate_blocks, block)
         up = blocks_dot(piece, up_blocks, block)
         if step:
@@ -210,25 +258,21 @@
         gates = gate if gates is None else gates + gate
         ups = up if ups is None else ups + up
     hidden = (jax.nn.silu(gates) * ups).astype(jnp.bfloat16)
+    received = [to_high(hidden, step, ranks) for step in range(highs)]
     terms = []
     for step in range(highs):
-        theirs = to_high(hidden, step, ranks)
-        terms += [
-            jnp.dot(theirs, weight, preferred_element_type=jnp.float32).astype(jnp.bfloat16)
-            for weight in down_blocks
-        ]
-    terms = lax.psum_scatter(
-        jnp.concatenate(terms, axis=1), "tp", scatter_dimension=0, tiled=True
-    )
-    terms = jnp.concatenate(
-        [
-            by_distance(
-                to_high(terms[:, step * wide : (step + 1) * wide], highs - step, ranks), place
-            )
-            for step in range(highs)
-        ],
-        axis=1,
-    )
+        partial = jnp.concatenate(
+            [
+                jnp.dot(received[step], weight, preferred_element_type=jnp.float32).astype(
+                    jnp.bfloat16
+                )
+                for weight in down_blocks
+            ],
+            axis=1,
+        )
+        partial = to_high(scatter_columns(partial), highs - step, ranks)
+        terms.append(by_distance(partial, place))
+    terms = jnp.concatenate(terms, axis=1)
     ffn_sum = jnp.concatenate(
         [
             lax.dynamic_slice_in_dim(terms, (index - high + highs) % highs * wide, wide, 1)

time: 434 us -> 356 us (0.82)
  waiting for transfers between devices: 317 us -> 218 us
  starting transfers between devices: 18.7 us -> 61 us
  matrix products: 56.9 us -> 36.9 us
  between operations: 13.7 us -> 0.97 us
  local copies, waits for them, and re-layouts: 6.87 us -> 14.3 us
    all_gather x2 -> x0, waiting for transfers between devices: 55.5 us -> none  [the longest x1 55.4 us: body(): lax.all_gather(jnp.concatenate([latent, rope_key], axis=1), 'sp', axis=0,...]
    ppermute x5, waiting for transfers between devices: 117 us -> 85.9 us  [to_high(): lax.ppermute(values, 'sp', [(rank, (rank + step * GROUP) % ranks) for ran...]
    reduce_scatter x2 -> x0, waiting for transfers between devices: 30.5 us -> none  [the longest x1 30.5 us: body(): lax.psum_scatter(jnp.concatenate(terms, axis=1), 'tp', scatter_dimension=...]
    ppermute x0 -> x19, waiting for transfers between devices: none -> 29.4 us  [the longest x12 23.7 us: to_column(): lax.ppermute(values, 'tp', [(column, column ^ bit) for column in range(co...]
    ppermute x0 -> x19, starting transfers between devices: none -> 25.3 us  [the longest x7 18.7 us: body(): pieces.append(lax.ppermute(both, 'sp', onward))]
    ppermute x10, starting transfers between devices: 11.5 us -> 27.8 us  [to_near(): lax.ppermute(values, 'sp', [(rank, rank ^ flip) for rank in range(ranks)])]
    ppermute x10, waiting for transfers between devices: 114 us -> 102 us  [to_near(): lax.ppermute(values, 'sp', [(rank, rank ^ flip) for rank in range(ranks)])]
    dot_general x16, matrix products: 29.5 us -> 20.7 us  [blocks_dot(): jnp.dot(rows[:, place * block:(place + 1) * block], weight, preferred_ele...]
  transfers between devices with their start and end apart: 19 -> 34, of which waited for: 13 -> 20; matrix products, arithmetic and copies ran while one was open for 9% -> 10% of each run, Pallas kernels for 0% -> 0%
where the time goes in v2:
time: 356 us; the launch traced here: 355 us
  waiting for transfers between devices  218 us (61%)
  starting transfers between devices  61 us (17%)
  matrix products  36.9 us (10%)
  other arithmetic  17.1 us (5%)
  local copies, waits for them, and re-layouts  14.3 us (4%)
  blocking collectives  6.89 us (2%)
    ppermute x10, waiting for transfers between devices, to_near(): lax.ppermute(values, 'sp', [(rank, rank ^ flip) for rank in range(ranks)])  102 us
    ppermute x5, waiting for transfers between devices, to_high(): lax.ppermute(values, 'sp', [(rank, (rank + step * GROUP) % ranks) for ran...  85.9 us
    ppermute x10, starting transfers between devices, to_near(): lax.ppermute(values, 'sp', [(rank, rank ^ flip) for rank in range(ranks)])  27.8 us
    ppermute x12, waiting for transfers between devices, to_column(): lax.ppermute(values, 'tp', [(column, column ^ bit) for column in range(co...  23.7 us
    dot_general x16, matrix products, blocks_dot(): jnp.dot(rows[:, place * block:(place + 1) * block], weight, preferred_ele...  20.7 us
    ppermute x7, starting transfers between devices, body(): pieces.append(lax.ppermute(both, 'sp', onward))  18.7 us
    ppermute x5, starting transfers between devices, to_high(): lax.ppermute(values, 'sp', [(rank, (rank + step * GROUP) % ranks) for ran...  7.86 us
  transfers between devices with their start and end apart: 34, of which 20 were waited for; matrix products, arithmetic and copies ran while one was open for 10% of the time, Pallas kernels for 0%

profile of v2, /device:TPU:0, one launch (start us, length us, event | category | flops | bytes accessed | tf_op | source)
XLA Modules:
  0.0 354.7 jit_solution(2480890601895744574)
XLA Ops:
  2.0 4.9 %collective-permute-start = (bf16[64,576]{0,1:T(8,128)(2,1)S(1)}, bf16[64,576]{0,1:T(8,128)(2,1)S(1)}, u32[]{:S(2)}, u32[]{:S(2)}) collective-permute-start(bf16[64,576]{0,1:T(8,128)(2,1)S(1)} %fusion.82), channel_id=1, source_target_pairs={{0,4},{4,8},{8,12},{12,16},{16,20},{20,24},{24,28},{1,5},{5,9},{9,... | collective-permute-start | bytes 221192 | tf_op jit(solution)/shard_map/ppermute | solution.py:207
  6.9 3.5 collective-permute-start.1
  10.4 4.5 %collective-permute-start.2 = (bf16[64,576]{0,1:T(8,128)(2,1)S(1)}, bf16[64,576]{0,1:T(8,128)(2,1)S(1)}, u32[]{:S(2)}, u32[]{:S(2)}) collective-permute-start(bf16[64,576]{0,1:T(8,128)(2,1)S(1)} %fusion.82), channel_id=1, source_target_pairs={{0,12},{4,16},{8,20},{12,24},{16,28},{1,13},{5,17},{9,21},{13,25},... | collective-permute-start | bytes 221192 | tf_op jit(solution)/shard_map/ppermute | solution.py:207
  25.2 3.2 collective-permute-done.5
  34.4 11.3 %collective-permute-done.7 = bf16[512,576]{0,1:T(8,128)(2,1)S(1)} collective-permute-done((bf16[512,576]{0,1:T(8,128)(2,1)}, bf16[512,576]{0,1:T(8,128)(2,1)S(1)}, u32[]{:S(2)}, u32[]{:S(2)}) %collective-permute-start.7) | collective-permute-done | bytes 589856 | tf_op jit(solution)/shard_map/ppermute | solution.py:77
  51.9 4.0 %concatenate.80 = bf16[2048,576]{0,1:T(8,128)(2,1)S(1)} concatenate(bf16[64,576]{0,1:T(8,128)(2,1)S(1)} %fusion.82, bf16[64,576]{0,1:T(8,128)(2,1)} %copy-done.6, bf16[64,576]{0,1:T(8,128)(2,1)} %copy-done.7, bf16[64,576]{0,1:T(8,128)(2,1)} %copy-done.8, bf16[64,576]{0,1:T(8,128)(2,1)} %copy-done.9, bf16[64,576]{0,1:T(8,128)(2,1)} %copy-done.10, bf16[64,576]{0,1:T(8,128)(2,1)} %copy-done.11, ...), dimensions={0} | concatenate | bytes 4718592 | tf_op jit(solution)/shard_map/concatenate | solution.py:90
  68.0 6.9 %psum.7 = f32[256]{0:T(256)S(1)} all-reduce(f32[256]{0:T(256)S(1)} %pad_maximum_fusion.12), channel_id=1, replica_groups=mesh['sp'=8,'tp'=4] {'tp'}, use_global_device_ids=true, to_apply=%region_4.5 | all-reduce | flops 256 | bytes 2048 | tf_op jit(solution)/shard_map/psum | solution.py:222
  75.2 3.5 convolution_convert_fusion
  79.0 6.9 %collective-permute-start.17 = (bf16[512,1536]{1,0:T(8,128)(2,1)}, bf16[512,1536]{1,0:T(8,128)(2,1)}, u32[]{:S(2)}, u32[]{:S(2)}) collective-permute-start(bf16[512,1536]{1,0:T(8,128)(2,1)} %param.22), channel_id=1, source_target_pairs={{0,8},{4,12},{8,0},{12,4},{16,24},{20,28},{24,16},{28,20},{1,9},{5... | collective-permute-start | bytes 4718600 | tf_op jit(solution)/shard_map/ppermute | solution.py:51
  87.7 28.4 %collective-permute-done.14 = bf16[512,1536]{1,0:T(8,128)(2,1)} collective-permute-done((bf16[512,1536]{1,0:T(8,128)(2,1)}, bf16[512,1536]{1,0:T(8,128)(2,1)}, u32[]{:S(2)}, u32[]{:S(2)}) %collective-permute-start.14) | collective-permute-done | bytes 1572896 | tf_op jit(solution)/shard_map/ppermute | solution.py:51
  116.1 6.9 %collective-permute-start.16 = (bf16[512,1536]{1,0:T(8,128)(2,1)}, bf16[512,1536]{1,0:T(8,128)(2,1)S(1)}, u32[]{:S(2)}, u32[]{:S(2)}) collective-permute-start(bf16[512,1536]{1,0:T(8,128)(2,1)} %collective-permute-done.14), channel_id=1, source_target_pairs={{0,8},{4,12},{8,0},{12,4},{16,24},{20,28},{24,16},{28,20},{1,9},{5... | collective-permute-start | bytes 4718600 | tf_op jit(solution)/shard_map/ppermute | solution.py:51
  127.6 3.2 collective-permute-start.11
  133.0 29.2 %collective-permute-done.11 = bf16[64,2048]{1,0:T(8,128)(2,1)S(1)} collective-permute-done((bf16[64,2048]{1,0:T(8,128)(2,1)S(1)}, bf16[64,2048]{1,0:T(8,128)(2,1)S(1)}, u32[]{:S(2)}, u32[]{:S(2)}) %collective-permute-start.11) | collective-permute-done | bytes 262176 | tf_op jit(solution)/shard_map/ppermute | solution.py:57
  162.9 3.9 %collective-permute-start.15 = (bf16[512,1536]{1,0:T(8,128)(2,1)}, bf16[512,1536]{1,0:T(8,128)(2,1)S(1)}, u32[]{:S(2)}, u32[]{:S(2)}) collective-permute-start(bf16[512,1536]{1,0:T(8,128)(2,1)} %param.21), channel_id=1, source_target_pairs={{0,8},{4,12},{8,0},{12,4},{16,24},{20,28},{24,16},{28,20},{1,9},{5... | collective-permute-start | bytes 4718600 | tf_op jit(solution)/shard_map/ppermute | solution.py:51
  169.1 4.7 %collective-permute-start.25 = (bf16[1536,512]{1,0:T(8,128)(2,1)S(1)}, bf16[1536,512]{1,0:T(8,128)(2,1)S(1)}, u32[]{:S(2)}, u32[]{:S(2)}) collective-permute-start(bf16[1536,512]{1,0:T(8,128)(2,1)S(1)} %copy-done.21), channel_id=1, source_target_pairs={{0,8},{4,12},{8,0},{12,4},{16,24},{20,28},{24,16},{28,20},{1,9},{5... | collective-permute-start | bytes 4718600 | tf_op jit(solution)/shard_map/ppermute | solution.py:51
  174.1 20.1 %collective-permute-done.22 = bf16[512,1536]{1,0:T(8,128)(2,1)S(1)} collective-permute-done((bf16[512,1536]{1,0:T(8,128)(2,1)}, bf16[512,1536]{1,0:T(8,128)(2,1)S(1)}, u32[]{:S(2)}, u32[]{:S(2)}) %collective-permute-start.22) | collective-permute-done | bytes 1572896 | tf_op jit(solution)/shard_map/ppermute | solution.py:51
  206.0 3.2 collective-permute-start.19
  217.0 9.1 %collective-permute-done.24 = bf16[1536,512]{1,0:T(8,128)(2,1)S(1)} collective-permute-done((bf16[1536,512]{1,0:T(8,128)(2,1)S(1)}, bf16[1536,512]{1,0:T(8,128)(2,1)S(1)}, u32[]{:S(2)}, u32[]{:S(2)}) %collective-permute-start.24) | collective-permute-done | bytes 1572896 | tf_op jit(solution)/shard_map/ppermute | solution.py:51
  226.6 37.0 %collective-permute-done.25 = bf16[1536,512]{1,0:T(8,128)(2,1)S(1)} collective-permute-done((bf16[1536,512]{1,0:T(8,128)(2,1)S(1)}, bf16[1536,512]{1,0:T(8,128)(2,1)S(1)}, u32[]{:S(2)}, u32[]{:S(2)}) %collective-permute-start.25) | collective-permute-done | bytes 1572896 | tf_op jit(solution)/shard_map/ppermute | solution.py:51
  265.8 9.1 %collective-permute-done.23 = bf16[256,1536]{1,0:T(8,128)(2,1)S(1)} collective-permute-done((bf16[256,1536]{1,0:T(8,128)(2,1)S(1)}, bf16[256,1536]{1,0:T(8,128)(2,1)S(1)}, u32[]{:S(2)}, u32[]{:S(2)}) %collective-permute-start.23) | collective-permute-done | bytes 786464 | tf_op jit(solution)/shard_map/ppermute | solution.py:57
  277.4 7.4 %collective-permute-done.26 = bf16[768,512]{1,0:T(8,128)(2,1)S(1)} collective-permute-done((bf16[768,512]{1,0:T(8,128)(2,1)S(1)}, bf16[768,512]{1,0:T(8,128)(2,1)S(1)}, u32[]{:S(2)}, u32[]{:S(2)}) %collective-permute-start.26) | collective-permute-done | bytes 786464 | tf_op jit(solution)/shard_map/ppermute | solution.py:51
  289.6 34.1 %collective-permute-done.30 = bf16[256,1536]{1,0:T(8,128)(2,1)S(1)} collective-permute-done((bf16[256,1536]{1,0:T(8,128)(2,1)S(1)}, bf16[256,1536]{1,0:T(8,128)(2,1)S(1)}, u32[]{:S(2)}, u32[]{:S(2)}) %collective-permute-start.30) | collective-permute-done | bytes 786464 | tf_op jit(solution)/shard_map/ppermute | solution.py:57
  332.0 6.7 %collective-permute-done.32 = bf16[64,2048]{1,0:T(8,128)(2,1)S(1)} collective-permute-done((bf16[64,2048]{1,0:T(8,128)(2,1)S(1)}, bf16[64,2048]{1,0:T(8,128)(2,1)S(1)}, u32[]{:S(2)}, u32[]{:S(2)}) %collective-permute-start.32) | collective-permute-done | bytes 262176 | tf_op jit(solution)/shard_map/ppermute | solution.py:77
  340.0 13.5 %collective-permute-done.33 = bf16[64,2048]{1,0:T(8,128)(2,1)S(1)} collective-permute-done((bf16[64,2048]{1,0:T(8,128)(2,1)S(1)}, bf16[64,2048]{1,0:T(8,128)(2,1)S(1)}, u32[]{:S(2)}, u32[]{:S(2)}) %collective-permute-start.33) | collective-permute-done | bytes 262176 | tf_op jit(solution)/shard_map/ppermute | solution.py:57
  (191 shorter events, 88.7 us)
Async XLA Ops:
  2.0 19.2 %collective-permute-start = (bf16[64,576]{0,1:T(8,128)(2,1)S(1)}, bf16[64,576]{0,1:T(8,128)(2,1)S(1)}, u32[]{:S(2)}, u32[]{:S(2)}) collective-permute-start(bf16[64,576]{0,1:T(8,128)(2,1)S(1)} %fusion.82), channel_id=1, source_target_pairs={{0,4},{4,8},{8,12},{12,16},{16,20},{20,24},{24,28},{1,5},{5,9},{9,... | collective-permute-start | bytes 221192 | tf_op jit(solution)/shard_map/ppermute | solution.py:207
  6.9 15.6 %collective-permute-start.1 = (bf16[64,576]{0,1:T(8,128)(2,1)S(1)}, bf16[64,576]{0,1:T(8,128)(2,1)S(1)}, u32[]{:S(2)}, u32[]{:S(2)}) collective-permute-start(bf16[64,576]{0,1:T(8,128)(2,1)S(1)} %fusion.82), channel_id=1, source_target_pairs={{0,8},{4,12},{8,16},{12,20},{16,24},{20,28},{1,9},{5,13},{9,17},{1... | collective-permute-start | bytes 221192 | tf_op jit(solution)/shard_map/ppermute | solution.py:207
  10.4 14.1 %collective-permute-start.2 = (bf16[64,576]{0,1:T(8,128)(2,1)S(1)}, bf16[64,576]{0,1:T(8,128)(2,1)S(1)}, u32[]{:S(2)}, u32[]{:S(2)}) collective-permute-start(bf16[64,576]{0,1:T(8,128)(2,1)S(1)} %fusion.82), channel_id=1, source_target_pairs={{0,12},{4,16},{8,20},{12,24},{16,28},{1,13},{5,17},{9,21},{13,25},... | collective-permute-start | bytes 221192 | tf_op jit(solution)/shard_map/ppermute | solution.py:207
  14.9 9.6 %collective-permute-start.3 = (bf16[64,576]{0,1:T(8,128)(2,1)S(1)}, bf16[64,576]{0,1:T(8,128)(2,1)S(1)}, u32[]{:S(2)}, u32[]{:S(2)}) collective-permute-start(bf16[64,576]{0,1:T(8,128)(2,1)S(1)} %fusion.82), channel_id=1, source_target_pairs={{0,16},{4,20},{8,24},{12,28},{1,17},{5,21},{9,25},{13,29},{2,18},{... | collective-permute-start | bytes 221192 | tf_op jit(solution)/shard_map/ppermute | solution.py:207
  31.4 14.2 %collective-permute-start.7 = (bf16[512,576]{0,1:T(8,128)(2,1)}, bf16[512,576]{0,1:T(8,128)(2,1)S(1)}, u32[]{:S(2)}, u32[]{:S(2)}) collective-permute-start(bf16[512,576]{0,1:T(8,128)(2,1)} %concatenate.78), channel_id=1, source_target_pairs={{0,2},{1,3},{2,0},{3,1},{4,6},{5,7},{6,4},{7,5},{8,10},{9,11},{10,... | collective-permute-start | bytes 1769480 | tf_op jit(solution)/shard_map/ppermute | solution.py:77
  79.0 37.1 %collective-permute-start.14 = (bf16[512,1536]{1,0:T(8,128)(2,1)}, bf16[512,1536]{1,0:T(8,128)(2,1)}, u32[]{:S(2)}, u32[]{:S(2)}) collective-permute-start(bf16[512,1536]{1,0:T(8,128)(2,1)} %param.21), channel_id=1, source_target_pairs={{0,4},{4,0},{8,12},{12,8},{16,20},{20,16},{24,28},{28,24},{1,5},{5... | collective-permute-start | bytes 4718600 | tf_op jit(solution)/shard_map/ppermute | solution.py:51
  79.0 43.9 %collective-permute-start.17 = (bf16[512,1536]{1,0:T(8,128)(2,1)}, bf16[512,1536]{1,0:T(8,128)(2,1)}, u32[]{:S(2)}, u32[]{:S(2)}) collective-permute-start(bf16[512,1536]{1,0:T(8,128)(2,1)} %param.22), channel_id=1, source_target_pairs={{0,8},{4,12},{8,0},{12,4},{16,24},{20,28},{24,16},{28,20},{1,9},{5... | collective-permute-start | bytes 4718600 | tf_op jit(solution)/shard_map/ppermute | solution.py:51
  87.1 36.1 %collective-permute-start.10 = (bf16[64,4096]{1,0:T(8,128)(2,1)S(1)}, bf16[64,4096]{1,0:T(8,128)(2,1)S(1)}, u32[]{:S(2)}, u32[]{:S(2)}) collective-permute-start(bf16[64,4096]{1,0:T(8,128)(2,1)S(1)} %add_convert_fusion.2), channel_id=1, source_target_pairs={{0,2},{1,3},{2,0},{3,1},{4,6},{5,7},{6,4},{7,5},{8,10},{9,11},{10,... | collective-permute-start | bytes 1572872 | tf_op jit(solution)/shard_map/ppermute | solution.py:77
  116.1 46.8 %collective-permute-start.16 = (bf16[512,1536]{1,0:T(8,128)(2,1)}, bf16[512,1536]{1,0:T(8,128)(2,1)S(1)}, u32[]{:S(2)}, u32[]{:S(2)}) collective-permute-start(bf16[512,1536]{1,0:T(8,128)(2,1)} %collective-permute-done.14), channel_id=1, source_target_pairs={{0,8},{4,12},{8,0},{12,4},{16,24},{20,28},{24,16},{28,20},{1,9},{5... | collective-permute-start | bytes 4718600 | tf_op jit(solution)/shard_map/ppermute | solution.py:51
  123.0 43.8 %collective-permute-start.18 = (bf16[512,1536]{1,0:T(8,128)(2,1)}, bf16[512,1536]{1,0:T(8,128)(2,1)S(1)}, u32[]{:S(2)}, u32[]{:S(2)}) collective-permute-start(bf16[512,1536]{1,0:T(8,128)(2,1)} %collective-permute-done.17), channel_id=1, source_target_pairs={{0,4},{4,0},{8,12},{12,8},{16,20},{20,16},{24,28},{28,24},{1,5},{5... | collective-permute-start | bytes 4718600 | tf_op jit(solution)/shard_map/ppermute | solution.py:51
  125.9 68.3 %collective-permute-start.22 = (bf16[512,1536]{1,0:T(8,128)(2,1)}, bf16[512,1536]{1,0:T(8,128)(2,1)S(1)}, u32[]{:S(2)}, u32[]{:S(2)}) collective-permute-start(bf16[512,1536]{1,0:T(8,128)(2,1)} %param.22), channel_id=1, source_target_pairs={{0,4},{4,0},{8,12},{12,8},{16,20},{20,16},{24,28},{28,24},{1,5},{5... | collective-permute-start | bytes 4718600 | tf_op jit(solution)/shard_map/ppermute | solution.py:51
  127.6 34.5 %collective-permute-start.11 = (bf16[64,2048]{1,0:T(8,128)(2,1)S(1)}, bf16[64,2048]{1,0:T(8,128)(2,1)S(1)}, u32[]{:S(2)}, u32[]{:S(2)}) collective-permute-start(bf16[64,2048]{1,0:T(8,128)(2,1)S(1)} %pad_maximum_fusion.10), channel_id=1, source_target_pairs={{0,16},{4,20},{8,24},{12,28},{16,0},{20,4},{24,8},{28,12},{1,17},{... | collective-permute-start | bytes 786440 | tf_op jit(solution)/shard_map/ppermute | solution.py:57
  132.9 40.9 %collective-permute-start.21 = (bf16[128,2048]{1,0:T(8,128)(2,1)S(1)}, bf16[128,2048]{1,0:T(8,128)(2,1)S(1)}, u32[]{:S(2)}, u32[]{:S(2)}) collective-permute-start(bf16[128,2048]{1,0:T(8,128)(2,1)S(1)} %pad_maximum_fusion.6), channel_id=1, source_target_pairs={{0,1},{1,0},{2,3},{3,2},{4,5},{5,4},{6,7},{7,6},{8,9},{9,8},{10,11... | collective-permute-start | bytes 1572872 | tf_op jit(solution)/shard_map/ppermute | solution.py:77
  162.9 41.9 %collective-permute-start.15 = (bf16[512,1536]{1,0:T(8,128)(2,1)}, bf16[512,1536]{1,0:T(8,128)(2,1)S(1)}, u32[]{:S(2)}, u32[]{:S(2)}) collective-permute-start(bf16[512,1536]{1,0:T(8,128)(2,1)} %param.21), channel_id=1, source_target_pairs={{0,8},{4,12},{8,0},{12,4},{16,24},{20,28},{24,16},{28,20},{1,9},{5... | collective-permute-start | bytes 4718600 | tf_op jit(solution)/shard_map/ppermute | solution.py:51
  166.8 59.4 %collective-permute-start.24 = (bf16[1536,512]{1,0:T(8,128)(2,1)S(1)}, bf16[1536,512]{1,0:T(8,128)(2,1)S(1)}, u32[]{:S(2)}, u32[]{:S(2)}) collective-permute-start(bf16[1536,512]{1,0:T(8,128)(2,1)S(1)} %copy-done.21), channel_id=1, source_target_pairs={{0,4},{4,0},{8,12},{12,8},{16,20},{20,16},{24,28},{28,24},{1,5},{5... | collective-permute-start | bytes 4718600 | tf_op jit(solution)/shard_map/ppermute | solution.py:51
  169.1 94.5 %collective-permute-start.25 = (bf16[1536,512]{1,0:T(8,128)(2,1)S(1)}, bf16[1536,512]{1,0:T(8,128)(2,1)S(1)}, u32[]{:S(2)}, u32[]{:S(2)}) collective-permute-start(bf16[1536,512]{1,0:T(8,128)(2,1)S(1)} %copy-done.21), channel_id=1, source_target_pairs={{0,8},{4,12},{8,0},{12,4},{16,24},{20,28},{24,16},{28,20},{1,9},{5... | collective-permute-start | bytes 4718600 | tf_op jit(solution)/shard_map/ppermute | solution.py:51
  173.8 26.8 %collective-permute-start.13 = (bf16[128,2048]{1,0:T(8,128)(2,1)S(1)}, bf16[128,2048]{1,0:T(8,128)(2,1)S(1)}, u32[]{:S(2)}, u32[]{:S(2)}) collective-permute-start(bf16[128,2048]{1,0:T(8,128)(2,1)S(1)} %pad_maximum_fusion.5), channel_id=1, source_target_pairs={{0,1},{1,0},{2,3},{3,2},{4,5},{5,4},{6,7},{7,6},{8,9},{9,8},{10,11... | collective-permute-start | bytes 1572872 | tf_op jit(solution)/shard_map/ppermute | solution.py:77
  206.0 59.2 %collective-permute-start.19 = (bf16[256,1536]{1,0:T(8,128)(2,1)S(1)}, bf16[256,1536]{1,0:T(8,128)(2,1)S(1)}, u32[]{:S(2)}, u32[]{:S(2)}) collective-permute-start(bf16[256,1536]{1,0:T(8,128)(2,1)S(1)} %fusion.14), channel_id=1, source_target_pairs={{0,16},{4,20},{8,24},{12,28},{16,0},{20,4},{24,8},{28,12},{1,17},{... | collective-permute-start | bytes 2359304 | tf_op jit(solution)/shard_map/ppermute | solution.py:57
  214.4 60.5 %collective-permute-start.23 = (bf16[256,1536]{1,0:T(8,128)(2,1)S(1)}, bf16[256,1536]{1,0:T(8,128)(2,1)S(1)}, u32[]{:S(2)}, u32[]{:S(2)}) collective-permute-start(bf16[256,1536]{1,0:T(8,128)(2,1)S(1)} %fusion.15), channel_id=1, source_target_pairs={{0,16},{4,20},{8,24},{12,28},{16,0},{20,4},{24,8},{28,12},{1,17},{... | collective-permute-start | bytes 2359304 | tf_op jit(solution)/shard_map/ppermute | solution.py:57
  226.2 58.6 %collective-permute-start.26 = (bf16[768,512]{1,0:T(8,128)(2,1)S(1)}, bf16[768,512]{1,0:T(8,128)(2,1)S(1)}, u32[]{:S(2)}, u32[]{:S(2)}) collective-permute-start(bf16[768,512]{1,0:T(8,128)(2,1)S(1)} %slice.136), channel_id=1, source_target_pairs={{0,8},{4,12},{8,0},{12,4},{16,24},{20,28},{24,16},{28,20},{1,9},{5... | collective-permute-start | bytes 2359304 | tf_op jit(solution)/shard_map/ppermute | solution.py:51
  263.6 21.2 %collective-permute-start.27 = (bf16[768,512]{1,0:T(8,128)(2,1)S(1)}, bf16[768,512]{1,0:T(8,128)(2,1)S(1)}, u32[]{:S(2)}, u32[]{:S(2)}) collective-permute-start(bf16[768,512]{1,0:T(8,128)(2,1)S(1)} %slice.137), channel_id=1, source_target_pairs={{0,4},{4,0},{8,12},{12,8},{16,20},{20,16},{24,28},{28,24},{1,5},{5... | collective-permute-start | bytes 2359304 | tf_op jit(solution)/shard_map/ppermute | solution.py:51
  286.0 37.7 %collective-permute-start.30 = (bf16[256,1536]{1,0:T(8,128)(2,1)S(1)}, bf16[256,1536]{1,0:T(8,128)(2,1)S(1)}, u32[]{:S(2)}, u32[]{:S(2)}) collective-permute-start(bf16[256,1536]{1,0:T(8,128)(2,1)S(1)} %multiply_convert_fusion), channel_id=1, source_target_pairs={{0,16},{4,20},{8,24},{12,28},{16,0},{20,4},{24,8},{28,12},{1,17},{... | collective-permute-start | bytes 2359304 | tf_op jit(solution)/shard_map/ppermute | solution.py:57
  288.0 39.1 %collective-permute-start.29 = (bf16[64,2048]{1,0:T(8,128)(2,1)S(1)}, bf16[64,2048]{1,0:T(8,128)(2,1)}, u32[]{:S(2)}, u32[]{:S(2)}) collective-permute-start(bf16[64,2048]{1,0:T(8,128)(2,1)S(1)} %add_convert_fusion.8), channel_id=1, source_target_pairs={{0,2},{1,3},{2,0},{3,1},{4,6},{5,7},{6,4},{7,5},{8,10},{9,11},{10,... | collective-permute-start | bytes 786440 | tf_op jit(solution)/shard_map/ppermute | solution.py:77
  339.8 13.6 %collective-permute-start.33 = (bf16[64,2048]{1,0:T(8,128)(2,1)S(1)}, bf16[64,2048]{1,0:T(8,128)(2,1)S(1)}, u32[]{:S(2)}, u32[]{:S(2)}) collective-permute-start(bf16[64,2048]{1,0:T(8,128)(2,1)S(1)} %add_convert_fusion.4), channel_id=1, source_target_pairs={{0,16},{4,20},{8,24},{12,28},{16,0},{20,4},{24,8},{28,12},{1,17},{... | collective-permute-start | bytes 786440 | tf_op jit(solution)/shard_map/ppermute | solution.py:57
  (33 other events, 388.3 us)
